TPU v7x, 32 devices: a whole 2x2x4 slice. The times are simulated.
32 devices in a mesh: sp: 8 (over z, y), tp: 4 (over x, core).
Axes of the slice: x: 2, y: 2, z: 4, core: 2. Of those that a mesh axis runs over, the one named last changes fastest.
Arguments:
- tokens: bfloat16 [4096, 2048], P('sp', 'tp'), may hold values from -400 to 400
- norm_gain: float32 [2048], replicated, may hold values from 0.1 to 1.9
- query_weight: bfloat16 [2048, 1024], P(None, 'tp'), may hold values from -0.37306796 to 0.37306796
- key_weight: bfloat16 [2048, 1024], P(None, 'tp'), may hold values from -0.2625825 to 0.2625825
- value_weight: bfloat16 [2048, 1024], P(None, 'tp'), may hold values from -0.125 to 0.125
- outer_gate_weight: bfloat16 [2048, 1024], P(None, 'tp'), may hold values from -0.125 to 0.125
- inner_gate_weight: bfloat16 [2048, 1024], P(None, 'tp'), may hold values from -0.125 to 0.125
- conv_input_weight: bfloat16 [2048, 1024], P(None, 'tp'), may hold values from -0.125 to 0.125
- conv_taps: float32 [3, 1024], P(None, 'tp'), may hold values from -3.5 to 3.5
- lambdas: float32 [8], P('tp'), may hold values from 0.3 to 0.8
- head_gain: float32 [128], replicated, may hold values from 0.1 to 1.9
- attn_out_weight: bfloat16 [1024, 2048], P(None, 'tp'), may hold values from -0.125 to 0.125
- conv_out_weight: bfloat16 [1024, 2048], P(None, 'tp'), may hold values from -0.125 to 0.125
Outputs:
- mixed_out: bfloat16 [4096, 2048], P('sp', 'tp')
- log_totals: float32 [8, 2, 4096], P('tp', None, 'sp')
All inputs are finite; a program needn't handle non-finite values.
Results may differ from a plain program's by a relative error of at most 0.014.
The roundings to bfloat16 on the way count: a program that leaves them out, or rounds other values in their place, can miss the bound.
Values may be sent and summed in bfloat16 or wider, within the bound.
A program may use at most 128 MiB of HBM per device.

v0:
```python
import math
import jax
import jax.numpy as jnp
from jax import lax
from jax.sharding import PartitionSpec as P

NORM_EPS = 1e-06
HEAD_EPS = 1e-05
ROPE_BASE = 500000.0
MASKED = -1e30
HEAD_SCALE = 0.8


def shifted(block, axis, distance):
    devices = range(lax.axis_size(axis))
    route = [(i - distance, i) for i in devices if i - distance in devices]
    return lax.ppermute(block, axis, route)


def rotate(field_in, positions):
    half_dim = field_in.shape[-1] // 2
    frequency = ROPE_BASE ** (-jnp.arange(half_dim, dtype=jnp.float32) * 2.0 / field_in.shape[-1])
    angles = positions[:, None] * frequency[None, :]
    cosine = jnp.cos(angles)[:, None, None, :]
    sine_part = jnp.sin(angles)[:, None, None, :]
    first_half = field_in[..., :half_dim]
    second_half = field_in[..., half_dim:]
    return jnp.concatenate(
        [
            first_half * cosine - second_half * sine_part,
            second_half * cosine + first_half * sine_part,
        ],
        axis=-1,
    )


def add_products(block_in, norm_gain, weights):
    floats = block_in.astype(jnp.float32)
    scaled = (floats * norm_gain[None, :]).astype(jnp.bfloat16)
    products = tuple(
        (jnp.dot(scaled, weight, preferred_element_type=jnp.float32) for weight in weights)
    )
    return (jnp.sum(floats * floats, axis=1, keepdims=True),) + products


def over_shards(step_fn, running, arrays, anchor, local_rows):
    shard_count = arrays[0].shape[0] // local_rows
    group_size = math.gcd(shard_count, max(1, 2048 // local_rows))
    block_rows = group_size * local_rows
    steps_count = shard_count // group_size
    stacked = tuple(
        (member.reshape((steps_count, block_rows) + member.shape[1:]) for member in arrays)
    )

    def scan_step(carried, scan_items):
        members, step_index = scan_items
        return (step_fn(carried, members, anchor + step_index * block_rows), None)

    result, unused = lax.scan(
        scan_step, running, (stacked, jnp.arange(steps_count, dtype=jnp.int32))
    )
    return result


def per_device(
    tokens,
    norm_gain,
    query_weight,
    key_weight,
    value_weight,
    outer_gate_weight,
    inner_gate_weight,
    conv_input_weight,
    conv_taps,
    lambdas,
    head_gain,
    attn_out_weight,
    conv_out_weight,
):
    local_rows = tokens.shape[0]
    local_heads = lambdas.shape[0]
    head_dim = query_weight.shape[1] // (2 * local_heads)
    value_dim = 2 * head_dim
    taps_count = conv_taps.shape[0]
    width_all = norm_gain.shape[0]
    columns_dev = query_weight.shape[1]
    attn_weights = (query_weight, key_weight, value_weight)
    conv_weights = (outer_gate_weight, inner_gate_weight, conv_input_weight)
    squares, query_raw, key_raw, value_raw, outer_raw, inner_raw, signal_raw = add_products(
        lax.all_gather(tokens, "tp", axis=1, tiled=True), norm_gain, attn_weights + conv_weights
    )
    inverse_rms = lax.rsqrt(squares / width_all + NORM_EPS)
    query_pos = lax.axis_index("sp") * local_rows + jnp.arange(local_rows, dtype=jnp.int32)
    positions = query_pos.astype(jnp.float32)
    queries = rotate(
        (inverse_rms * query_raw).reshape(local_rows, local_heads, 2, head_dim), positions
    ).astype(jnp.bfloat16)
    key_rows = rotate(
        (inverse_rms * key_raw).reshape(local_rows, local_heads, 2, head_dim), positions
    ).astype(jnp.bfloat16)
    values = (
        (inverse_rms * value_raw).astype(jnp.bfloat16).reshape(local_rows, local_heads, value_dim)
    )
    outer_gate = (inverse_rms * outer_raw).astype(jnp.bfloat16)
    inner_gate = (inverse_rms * inner_raw).astype(jnp.bfloat16)
    signal = (inverse_rms * signal_raw).astype(jnp.bfloat16)
    conv_in = (inner_gate.astype(jnp.float32) * signal.astype(jnp.float32)).astype(jnp.bfloat16)
    rim_rows = shifted(conv_in[local_rows - (taps_count - 1) :], "sp", 1)
    padded = jnp.concatenate([rim_rows, conv_in], axis=0)
    summed = jnp.zeros((local_rows, columns_dev), jnp.float32)
    for tap_index in range(taps_count):
        summed = summed + conv_taps[tap_index][None, :] * padded[
            tap_index : tap_index + local_rows
        ].astype(jnp.float32)
    conv_out = (outer_gate.astype(jnp.float32) * summed).astype(jnp.bfloat16)
    scale_factor = head_dim ** (-0.5)

    def block_scores(key_block, key_anchor):
        scores = (
            jnp.einsum("qhcd,khcd->hcqk", queries, key_block, preferred_element_type=jnp.float32)
            * scale_factor
        )
        visible = (
            query_pos[:, None]
            >= (key_anchor + jnp.arange(key_block.shape[0], dtype=jnp.int32))[None, :]
        )
        return (jnp.where(visible, scores, MASKED), visible)

    def stats_step(running, members, key_anchor):
        max_before, sum_before = running
        scores, visible = block_scores(members[0], key_anchor)
        max_after = jnp.maximum(max_before, jnp.max(scores, axis=-1))
        exponent = jnp.where(visible, jnp.exp(scores - max_after[..., None]), 0.0)
        return (
            max_after,
            sum_before * jnp.exp(max_before - max_after) + jnp.sum(exponent, axis=-1),
        )

    stats_init = (
        jnp.full((local_heads, 2, local_rows), MASKED, jnp.float32),
        jnp.zeros((local_heads, 2, local_rows), jnp.float32),
    )
    value_init = jnp.zeros((local_rows, local_heads, value_dim), jnp.float32)

    def value_step_with(row_max, row_sum):

        def value_step(running, members, key_anchor):
            scores, visible = block_scores(members[0], key_anchor)
            normalized = jnp.where(
                visible, jnp.exp(scores - row_max[..., None]) / row_sum[..., None], 0.0
            )
            weights = (normalized[:, 0] - lambdas[:, None, None] * normalized[:, 1]).astype(
                jnp.bfloat16
            )
            return running + jnp.einsum(
                "hqk,khv->qhv", weights, members[1], preferred_element_type=jnp.float32
            )

        return value_step

    all_keys, all_values = (
        lax.all_gather(key_rows, "sp", axis=0, tiled=True),
        lax.all_gather(values, "sp", axis=0, tiled=True),
    )
    row_max, row_sum = over_shards(stats_step, stats_init, (all_keys,), 0, local_rows)
    head_mix = over_shards(
        value_step_with(row_max, row_sum), value_init, (all_keys, all_values), 0, local_rows
    )
    log_totals = row_max + jnp.log(row_sum)
    normed = (
        head_mix
        * lax.rsqrt(jnp.mean(head_mix * head_mix, axis=-1, keepdims=True) + HEAD_EPS)
        * head_gain[None, None, :]
        * HEAD_SCALE
    )
    attn_out = normed.astype(jnp.bfloat16).reshape(local_rows, local_heads * value_dim)
    running = jnp.zeros((local_rows, attn_out_weight.shape[1]), jnp.float32)
    running = jnp.dot(
        lax.all_gather(attn_out, "tp", axis=1, tiled=True),
        attn_out_weight,
        preferred_element_type=jnp.float32,
    )
    mixed_out = running + jnp.dot(
        lax.all_gather(conv_out, "tp", axis=1, tiled=True),
        conv_out_weight,
        preferred_element_type=jnp.float32,
    )
    return (mixed_out.astype(jnp.bfloat16), log_totals)


def solution(mesh):
    in_specs = (
        P("sp", "tp"),
        P(),
        P(None, "tp"),
        P(None, "tp"),
        P(None, "tp"),
        P(None, "tp"),
        P(None, "tp"),
        P(None, "tp"),
        P(None, "tp"),
        P("tp"),
        P(),
        P(None, "tp"),
        P(None, "tp"),
    )
    out_specs = (P("sp", "tp"), P("tp", None, "sp"))
    return jax.shard_map(
        per_device, mesh=mesh, in_specs=in_specs, out_specs=out_specs, check_vma=False
    )
```

profile of v0, /device:TPU:0, one launch (start us, length us, event | category | flops | bytes accessed | tf_op | source)
XLA Modules:
  0.0 211.2 jit_solution(9740739602610465239)
XLA Ops:
  7.2 0.0 copy-start
  7.2 0.0 copy-start.16
  7.2 0.0 all-gather.6.cloned.1.call-start
  7.2 0.7 all-gather.6.cloned.1.call-update
  7.9 0.0 all-gather.10.cloned.1.call-start
  8.0 0.3 multiply_cosine_fusion
  8.3 26.6 %all-gather.6.cloned.1.call-done = bf16[512,2048]{1,0:T(8,128)(2,1)} async-done(((bf16[512,512]{1,0:T(8,128)(2,1)}), bf16[512,2048]{1,0:T(8,128)(2,1)}) %all-gather.6.cloned.1.call-update) | async-done | bytes 2097168 | tf_op jit(solution)/shard_map/all_gather | solution.py:90
  34.9 2.2 %fusion.32 = f32[512]{0:T(512)S(1)} fusion(bf16[512,2048]{1,0:T(8,128)(2,1)} %all-gather.6.cloned.1.call-done), kind=kLoop, calls=%fused_computation.40 | loop fusion | flops 3145216 | bytes 2099200 | tf_op jit(solution)/shard_map/reduce_sum | solution.py:43
  37.1 2.6 %convolution_multiply_fusion.4 = f32[512,256]{0,1:T(8,128)S(1)} fusion(bf16[2048,256]{1,0:T(8,128)(2,1)} %param.20, bf16[512,2048]{1,0:T(8,128)(2,1)} %all-gather.6.cloned.1.call-done, f32[2048]{0:T(1024)} %param.18, f32[512]{0:T(512)S(1)} %add_rsqrt_fusion.1), kind=kOutput, calls=%fused_computation.49 | convolution fusion | flops 540147712 | bytes 3680256 | tf_op jit(solution)/shard_map/dot_general | solution.py:41
  39.8 0.8 convolution_multiply_fusion.3
  40.6 0.2 subtract_convert_fusion
  40.8 0.7 pad_maximum_fusion.1
  41.5 0.0 all-gather.10.cloned.1.call-update
  41.5 0.0 all-gather.8.cloned.1.call-start
  41.6 2.7 %fusion.35 = bf16[512,256]{0,1:T(8,128)(2,1)} fusion(bf16[2048,256]{1,0:T(8,128)(2,1)} %param.21, bf16[512,2048]{1,0:T(8,128)(2,1)S(1)} %copy-done.1, f32[2048]{0:T(1024)} %param.18, f32[512]{0:T(512)S(1)} %add_rsqrt_fusion.1), kind=kOutput, calls=%fused_computation.51 | convolution fusion | flops 540278784 | bytes 3418112 | tf_op jit(solution)/shard_map/dot_general | solution.py:41
  44.3 1.8 copy.21
  46.1 0.0 all-gather.8.cloned.1.call-update
  46.1 0.0 all-gather.12.cloned.1.call-start
  46.2 0.7 pad_maximum_fusion.2
  46.9 45.2 %all-gather.10.cloned.1.call-done = bf16[4096,2,2,64]{0,3,2,1:T(8,128)(2,1)} async-done(((bf16[512,2,2,64]{0,3,2,1:T(8,128)(2,1)}), bf16[4096,2,2,64]{0,3,2,1:T(8,128)(2,1)}) %all-gather.10.cloned.1.call-update) | async-done | bytes 2097168 | tf_op jit(solution)/shard_map/all_gather | solution.py:162
  92.1 1.7 copy.34
  93.8 0.0 copy-start.18
  93.8 18.6 %while.24 = (s32[]{:T(128)}, f32[2,2,512]{2,1,0:T(2,128)S(1)}, f32[2,2,512]{2,1,0:T(2,128)S(1)}, s32[2]{0:T(128)S(1)}, bf16[2,2048,2,2,64]{1,4,3,2,0:T(8,128)(2,...) while((s32[]{:T(128)}, f32[2,2,512]{2,1,0:T(2,128)S(1)}, ...), condition=%wide.region_4.5_spmd.clone, body=%wide.region_1.4_spmd.clone.sunk | while | flops 571486720 | bytes 38138008 | solution.py:59
  93.8 0.6 dynamic_slice.43
  95.1 0.8 broadcast_compare_fusion.4
  95.9 3.0 %fusion.78 = (f32[2,2,512]{2,1,0:T(2,128)S(1)}, f32[2,2,2048,512]{3,2,1,0:T(8,128)S(1)}) fusion(pred[512,2048]{0,1:T(8,128)(4,1)S(1)} %broadcast_compare_fusion.4, bf16[512,2,2,64]{0,3,2,1:T(8,128)(2,1)S(1)} %get-tuple-element.355, bf16[2,2048,2,2,64]{1,4,3,2,0:T(8,128)(2,1)S(1)} %get-tuple-element.354, s32[]{:T(128)S(6)} %copy.38), kind=kOutput, calls=%fused_computation.4.clone.1 | convolution fusion | flops 549451776 | bytes 19144708 | tf_op jit(solution)/shard_map/while/body/eval_jaxpr/qhcd,khcd->hcqk/dot_general | solution.py:120
  98.9 4.2 %select_reduce_fusion.2 = f32[2,2,512]{2,1,0:T(2,128)S(1)} fusion(f32[2,2,2048,512]{3,2,1,0:T(8,128)S(1)} %get-tuple-element.319, f32[2,2,512]{2,1,0:T(2,128)S(1)} %fusion.79, pred[512,2048]{0,1:T(8,128)(4,1)S(1)} %broadcast_compare_fusion.4), kind=kLoop, calls=%fused_computation.3.clone.1 | loop fusion | flops 20969472 | bytes 17842176 | tf_op jit(solution)/shard_map/while/body/eval_jaxpr/reduce_sum | solution.py:136
  103.2 0.6 dynamic_slice.43
  104.5 0.8 broadcast_compare_fusion.4
  105.2 3.0 %fusion.78 = (f32[2,2,512]{2,1,0:T(2,128)S(1)}, f32[2,2,2048,512]{3,2,1,0:T(8,128)S(1)}) fusion(pred[512,2048]{0,1:T(8,128)(4,1)S(1)} %broadcast_compare_fusion.4, bf16[512,2,2,64]{0,3,2,1:T(8,128)(2,1)S(1)} %get-tuple-element.355, bf16[2,2048,2,2,64]{1,4,3,2,0:T(8,128)(2,1)S(1)} %get-tuple-element.354, s32[]{:T(128)S(6)} %copy.38), kind=kOutput, calls=%fused_computation.4.clone.1 | convolution fusion | flops 549451776 | bytes 19144708 | tf_op jit(solution)/shard_map/while/body/eval_jaxpr/qhcd,khcd->hcqk/dot_general | solution.py:120
  108.2 4.2 %select_reduce_fusion.2 = f32[2,2,512]{2,1,0:T(2,128)S(1)} fusion(f32[2,2,2048,512]{3,2,1,0:T(8,128)S(1)} %get-tuple-element.319, f32[2,2,512]{2,1,0:T(2,128)S(1)} %fusion.79, pred[512,2048]{0,1:T(8,128)(4,1)S(1)} %broadcast_compare_fusion.4), kind=kLoop, calls=%fused_computation.3.clone.1 | loop fusion | flops 20969472 | bytes 17842176 | tf_op jit(solution)/shard_map/while/body/eval_jaxpr/reduce_sum | solution.py:136
  112.5 29.0 %all-gather.8.cloned.1.call-done = bf16[4096,2,128]{2,0,1:T(8,128)(2,1)} async-done(((bf16[512,2,128]{2,0,1:T(8,128)(2,1)}), bf16[4096,2,128]{2,0,1:T(8,128)(2,1)}) %all-gather.8.cloned.1.call-update) | async-done | bytes 2097168 | tf_op jit(solution)/shard_map/all_gather | solution.py:163
  141.6 0.0 copy-start.9
  141.6 0.0 copy-start.17
  141.6 23.3 %while.25 = (s32[]{:T(128)}, f32[512,2,128]{0,2,1:T(8,128)}, bf16[2,2048,2,128]{3,1,0,2:T(8,128)(2,1)}, s32[2]{0:T(128)S(1)}, bf16[2,2048,2,2,64]{1,4,3,2,0:T(8,...) while((s32[]{:T(128)}, f32[512,2,128]{0,2,1:T(8,128)}, ...), condition=%wide.region_6.7_spmd.clone, body=%wide.region_5.6_spmd.clone.sunk | while | flops 1102318080 | bytes 51680008 | solution.py:59
  141.6 0.6 dynamic_slice.46
  142.9 0.8 broadcast_compare_fusion.5
  143.6 0.0 copy-start.4
  143.7 7.4 %fusion.85 = f32[2,2,512,2048]{2,3,1,0:T(8,128)S(1)} fusion(f32[2,2,512]{2,1,0:T(2,128)S(1)} %get-tuple-element.393, f32[2,2,512]{2,1,0:T(2,128)S(1)} %get-tuple-element.392, pred[512,2048]{0,1:T(8,128)(4,1)S(1)} %broadcast_compare_fusion.5, bf16[512,2,2,64]{0,3,2,1:T(8,128)(2,1)S(1)} %get-tuple-element.391, ...), kind=kOutput, calls=%fused_computation.20.clone.1 | convolution fusion | flops 557842432 | bytes 19152900 | tf_op jit(solution)/shard_map/while/body/eval_jaxpr/qhcd,khcd->hcqk/dot_general | solution.py:120
  151.1 1.3 fusion.86
  152.4 0.8 copy-done.5
  153.2 0.6 dynamic_slice.46
  154.5 0.8 broadcast_compare_fusion.5
  155.3 0.0 copy-start.4
  155.3 7.4 %fusion.85 = f32[2,2,512,2048]{2,3,1,0:T(8,128)S(1)} fusion(f32[2,2,512]{2,1,0:T(2,128)S(1)} %get-tuple-element.393, f32[2,2,512]{2,1,0:T(2,128)S(1)} %get-tuple-element.392, pred[512,2048]{0,1:T(8,128)(4,1)S(1)} %broadcast_compare_fusion.5, bf16[512,2,2,64]{0,3,2,1:T(8,128)(2,1)S(1)} %get-tuple-element.391, ...), kind=kOutput, calls=%fused_computation.20.clone.1 | convolution fusion | flops 557842432 | bytes 19152900 | tf_op jit(solution)/shard_map/while/body/eval_jaxpr/qhcd,khcd->hcqk/dot_general | solution.py:120
  162.7 1.3 fusion.86
  164.1 0.0 copy-start.5
  164.1 0.8 copy-done.5
  164.9 1.1 multiply_reduce_fusion
  166.0 1.9 multiply_convert_fusion
  167.8 0.0 all-gather.12.cloned.1.call-update
  167.9 0.2 all-gather.14.cloned.1.call-start
  168.2 2.1 %fusion.42 = f32[512,256]{0,1:T(8,128)S(1)} fusion(bf16[2048,256]{1,0:T(8,128)(2,1)} %param.23, bf16[512,2048]{1,0:T(8,128)(2,1)S(1)} %copy-done.2, f32[2048]{0:T(1024)S(1)} %copy-done.17, f32[512]{0:T(512)S(1)} %copy-done.9), kind=kOutput, calls=%fused_computation.58 | convolution fusion | flops 540409856 | bytes 3680256 | tf_op jit(solution)/shard_map/dot_general | solution.py:41
  170.3 0.8 fusion.41
  171.1 0.1 slice.54
  171.2 2.5 %collective-permute-start = (bf16[2,256]{0,1:T(8,128)(2,1)S(1)}, bf16[2,256]{0,1:T(8,128)(2,1)S(1)}, u32[]{:S(2)}, u32[]{:S(2)}) collective-permute-start(bf16[2,256]{0,1:T(8,128)(2,1)S(1)} %slice.54), channel_id=1, source_target_pairs={{0,4},{4,8},{8,12},{12,16},{16,20},{20,24},{24,28},{1,5},{5,9},{9,... | collective-permute-start | bytes 3080 | tf_op jit(solution)/shard_map/ppermute | solution.py:17
  173.7 1.9 collective-permute-done
  175.5 1.6 fusion.45
  177.2 0.0 all-gather.14.cloned.1.call-update
  177.2 0.6 log_add_fusion
  177.8 5.5 %all-gather.12.cloned.1.call-done = bf16[512,1024]{0,1:T(8,128)(2,1)} async-done(((bf16[512,256]{0,1:T(8,128)(2,1)}), bf16[512,1024]{0,1:T(8,128)(2,1)}) %all-gather.12.cloned.1.call-update) | async-done | bytes 1048592 | tf_op jit(solution)/shard_map/all_gather | solution.py:179
  183.3 2.0 fusion.54
  185.2 16.8 %all-gather.14.cloned.1.call-done = bf16[512,1024]{0,1:T(8,128)(2,1)} async-done(((bf16[512,256]{0,1:T(8,128)(2,1)}), bf16[512,1024]{0,1:T(8,128)(2,1)}) %all-gather.14.cloned.1.call-update) | async-done | bytes 1048592 | tf_op jit(solution)/shard_map/all_gather | solution.py:184
  202.0 2.8 %fusion.34 = bf16[512,512]{1,0:T(8,128)(2,1)} fusion(f32[512,512]{1,0:T(8,128)S(1)} %fusion.54, bf16[512,1024]{0,1:T(8,128)(2,1)} %all-gather.14.cloned.1.call-done, bf16[1024,512]{1,0:T(8,128)(2,1)S(1)} %copy-done.15), kind=kOutput, calls=%fused_computation.44 | convolution fusion | flops 537395200 | bytes 3670016 | tf_op jit(solution)/shard_map/dot_general | solution.py:183
  (58 shorter events, 0.3 us)
Async XLA Ops:
  7.2 176.1 %copy-start = (bf16[1024,512]{1,0:T(8,128)(2,1)S(1)}, bf16[1024,512]{1,0:T(8,128)(2,1)}, u32[]{:S(2)}) copy-start(bf16[1024,512]{1,0:T(8,128)(2,1)} %param.28) | copy-start | bytes 3145732
  7.2 32.6 %copy-start.16 = (f32[2048]{0:T(1024)S(1)}, f32[2048]{0:T(1024)}, u32[]{:S(2)}) copy-start(f32[2048]{0:T(1024)} %param.18) | copy-start | bytes 24580
  7.2 27.7 %all-gather.6.cloned.1.call-start = ((), (), s32[]{:S(2)}) async-start(), calls=%async_computation | async-start | bytes 2621440 | tf_op jit(solution)/shard_map/all_gather | solution.py:90
  7.9 84.1 %all-gather.10.cloned.1.call-start = ((), (), s32[]{:S(2)}) async-start(), calls=%async_computation.2 | async-start | bytes 2359296 | tf_op jit(solution)/shard_map/all_gather | solution.py:162
  34.9 4.9 %copy-start.1 = (bf16[512,2048]{1,0:T(8,128)(2,1)S(1)}, bf16[512,2048]{1,0:T(8,128)(2,1)}, u32[]{:S(2)}) copy-start(bf16[512,2048]{1,0:T(8,128)(2,1)} %all-gather.6.cloned.1.call-done) | copy-start | bytes 6291460
  34.9 4.9 %copy-start.12 = (bf16[2048,256]{1,0:T(8,128)(2,1)S(1)}, bf16[2048,256]{1,0:T(8,128)(2,1)}, u32[]{:S(2)}) copy-start(bf16[2048,256]{1,0:T(8,128)(2,1)} %param.19) | copy-start | bytes 3145732
  37.1 4.5 %copy-start.8 = (f32[512]{0:T(512)}, f32[512]{0:T(512)S(1)}, u32[]{:S(2)}) copy-start(f32[512]{0:T(512)S(1)} %add_rsqrt_fusion.1) | copy-start | bytes 6148
  41.5 100.0 %all-gather.8.cloned.1.call-start = ((), (), s32[]{:S(2)}) async-start(), calls=%async_computation.1 | async-start | bytes 2359296 | tf_op jit(solution)/shard_map/all_gather | solution.py:163
  46.1 137.1 %all-gather.12.cloned.1.call-start = ((), (), s32[]{:S(2)}) async-start(), calls=%async_computation.3 | async-start | bytes 1310720 | tf_op jit(solution)/shard_map/all_gather | solution.py:179
  46.9 46.9 %copy-start.6 = (bf16[512,2,2,64]{0,3,2,1:T(8,128)(2,1)S(1)}, bf16[512,2,2,64]{0,3,2,1:T(8,128)(2,1)}, u32[]{:S(2)}) copy-start(bf16[512,2,2,64]{0,3,2,1:T(8,128)(2,1)} %pad_maximum_fusion.2) | copy-start | bytes 786436
  93.8 47.7 %copy-start.18 = (f32[2]{0:T(128)S(1)}, f32[2]{0:T(128)}, u32[]{:S(2)}) copy-start(f32[2]{0:T(128)} %param.26) | copy-start | bytes 28
  112.5 29.1 %copy-start.3 = (bf16[2,2048,2,2,64]{1,4,3,2,0:T(8,128)(2,1)}, bf16[2,2048,2,2,64]{1,4,3,2,0:T(8,128)(2,1)S(1)}, u32[]{:S(2)}) copy-start(bf16[2,2048,2,2,64]{1,4,3,2,0:T(8,128)(2,1)S(1)} %get-tuple-element.405) | copy-start | bytes 6291460
  141.5 24.4 %copy-start.10 = (f32[128]{0:T(128)S(1)}, f32[128]{0:T(128)}, u32[]{:S(2)}) copy-start(f32[128]{0:T(128)} %param.27) | copy-start | bytes 1540
  141.5 26.6 %copy-start.2 = (bf16[512,2048]{1,0:T(8,128)(2,1)S(1)}, bf16[512,2048]{1,0:T(8,128)(2,1)}, u32[]{:S(2)}) copy-start(bf16[512,2048]{1,0:T(8,128)(2,1)} %all-gather.6.cloned.1.call-done) | copy-start | bytes 6291460
  141.6 26.6 %copy-start.9 = (f32[512]{0:T(512)S(1)}, f32[512]{0:T(512)}, u32[]{:S(2)}) copy-start(f32[512]{0:T(512)} %copy-done.8) | copy-start | bytes 6148
  141.6 26.6 %copy-start.17 = (f32[2048]{0:T(1024)S(1)}, f32[2048]{0:T(1024)}, u32[]{:S(2)}) copy-start(f32[2048]{0:T(1024)} %param.18) | copy-start | bytes 24580
  143.6 7.5 %copy-start.4 = (f32[512,2,128]{0,2,1:T(8,128)S(1)}, f32[512,2,128]{0,2,1:T(8,128)}, u32[]{:S(2)}) copy-start(f32[512,2,128]{0,2,1:T(8,128)} %get-tuple-element.374) | copy-start | bytes 1572868 | tf_op jit(solution)/shard_map/while
  143.7 7.5 %copy-start.11 = (bf16[2,2048,2,128]{3,1,0,2:T(8,128)(2,1)S(1)}, bf16[2,2048,2,128]{3,1,0,2:T(8,128)(2,1)}, u32[]{:S(2)}) copy-start(bf16[2,2048,2,128]{3,1,0,2:T(8,128)(2,1)} %get-tuple-element.388) | copy-start | bytes 6291460 | tf_op jit(solution)/shard_map/while
  152.4 0.8 copy-start.5
  155.3 7.4 %copy-start.4 = (f32[512,2,128]{0,2,1:T(8,128)S(1)}, f32[512,2,128]{0,2,1:T(8,128)}, u32[]{:S(2)}) copy-start(f32[512,2,128]{0,2,1:T(8,128)} %get-tuple-element.374) | copy-start | bytes 1572868 | tf_op jit(solution)/shard_map/while
  155.3 7.4 %copy-start.11 = (bf16[2,2048,2,128]{3,1,0,2:T(8,128)(2,1)S(1)}, bf16[2,2048,2,128]{3,1,0,2:T(8,128)(2,1)}, u32[]{:S(2)}) copy-start(bf16[2,2048,2,128]{3,1,0,2:T(8,128)(2,1)} %get-tuple-element.388) | copy-start | bytes 6291460 | tf_op jit(solution)/shard_map/while
  164.1 0.8 copy-start.5
  167.9 5.8 %copy-start.7 = (f32[3,256]{1,0:T(4,128)S(1)}, f32[3,256]{1,0:T(4,128)}, u32[]{:S(2)}) copy-start(f32[3,256]{1,0:T(4,128)} %param.25) | copy-start | bytes 9220
  167.9 34.1 %all-gather.14.cloned.1.call-start = ((), (), s32[]{:S(2)}) async-start(), calls=%async_computation.4 | async-start | bytes 1310720 | tf_op jit(solution)/shard_map/all_gather | solution.py:184
  168.1 2.2 %copy-start.13 = (bf16[2048,256]{1,0:T(8,128)(2,1)S(1)}, bf16[2048,256]{1,0:T(8,128)(2,1)}, u32[]{:S(2)}) copy-start(bf16[2048,256]{1,0:T(8,128)(2,1)} %param.24) | copy-start | bytes 3145732
  168.2 7.4 %copy-start.14 = (bf16[2048,256]{1,0:T(8,128)(2,1)S(1)}, bf16[2048,256]{1,0:T(8,128)(2,1)}, u32[]{:S(2)}) copy-start(bf16[2048,256]{1,0:T(8,128)(2,1)} %param.22) | copy-start | bytes 3145732
  171.2 4.3 %collective-permute-start = (bf16[2,256]{0,1:T(8,128)(2,1)S(1)}, bf16[2,256]{0,1:T(8,128)(2,1)S(1)}, u32[]{:S(2)}, u32[]{:S(2)}) collective-permute-start(bf16[2,256]{0,1:T(8,128)(2,1)S(1)} %slice.54), channel_id=1, source_target_pairs={{0,4},{4,8},{8,12},{12,16},{16,20},{20,24},{24,28},{1,5},{5,9},{9,... | collective-permute-start | bytes 3080 | tf_op jit(solution)/shard_map/ppermute | solution.py:17
  177.2 24.8 %copy-start.15 = (bf16[1024,512]{1,0:T(8,128)(2,1)S(1)}, bf16[1024,512]{1,0:T(8,128)(2,1)}, u32[]{:S(2)}) copy-start(bf16[1024,512]{1,0:T(8,128)(2,1)} %param.29) | copy-start | bytes 3145732
Sparse Core Ops, SparseCore 0:
  9.6 25.2 all-gather.5
  41.6 50.3 all-gather.9
  94.2 47.2 all-gather.7
  168.0 15.2 all-gather.11
  185.2 16.6 all-gather.13
where the time goes:
time: 212 us; the launch traced here: 211 us
  waiting for transfers between devices  126 us (59%)
  matrix products  38.8 us (18%)
  other arithmetic  19.3 us (9%)
  between operations  14.1 us (7%)
  local copies, waits for them, and re-layouts  7.83 us (4%)
  starting transfers between devices  2.84 us (1%)
  loops' own time  2.83 us (1%)
    all_gather x1, waiting for transfers between devices, per_device(): lax.all_gather(key_rows, 'sp', axis=0, tiled=True)  45.2 us
    all_gather x1, waiting for transfers between devices, per_device(): lax.all_gather(values, 'sp', axis=0, tiled=True)  29 us
    all_gather x1, waiting for transfers between devices, per_device(): lax.all_gather(tokens, 'tp', axis=1, tiled=True)  26.6 us
    dot_general x4, matrix products, block_scores(): jnp.einsum('qhcd,khcd->hcqk', queries, key_block, preferred_element_type=...  20.8 us
    all_gather x1, waiting for transfers between devices, per_device(): lax.all_gather(conv_out, 'tp', axis=1, tiled=True)  16.8 us
    dot_general x6, matrix products, add_products(): jnp.dot(scaled, weight, preferred_element_type=jnp.float32)  10.6 us
    reduce_sum x2, other arithmetic, stats_step(): jnp.sum(exponent, axis=-1)  8.38 us
    all_gather x1, waiting for transfers between devices, per_device(): lax.all_gather(attn_out, 'tp', axis=1, tiled=True)  5.45 us
  transfers between devices with their start and end apart: 6, of which 6 were waited for; matrix products, arithmetic and copies ran while one was open for 15% of the time, Pallas kernels for 0%

commit v1 on v0

--- a/solution.py
+++ b/solution.py
@@ -181,7 +181,7 @@
         preferred_element_type=jnp.float32,
     )
     mixed_out = running + jnp.dot(
-        lax.all_gather(conv_out, "tp", axis=1, tiled=True),
+        jnp.concatenate(lax.all_gather(conv_out, "tp"), axis=1),
         conv_out_weight,
         preferred_element_type=jnp.float32,
     )

time: 212 us -> 190 us (0.90)
  waiting for transfers between devices: 126 us -> 106 us
  matrix products: 38.8 us -> 34.3 us
    all_gather x1, waiting for transfers between devices: 16.8 us -> 0.02 us  [per_device(): lax.all_gather(conv_out, 'tp')]
    all_gather x1, waiting for transfers between devices: 45.2 us -> 35 us  [per_device(): lax.all_gather(key_rows, 'sp', axis=0, tiled=True)]
    all_gather x1, waiting for transfers between devices: 5.45 us -> 13.4 us  [per_device(): lax.all_gather(attn_out, 'tp', axis=1, tiled=True)]
    dot_general x4, matrix products: 20.8 us -> 17.6 us  [block_scores(): jnp.einsum('qhcd,khcd->hcqk', queries, key_block, preferred_element_type=...]
  transfers between devices with their start and end apart: 6 -> 6, of which waited for: 6 -> 5; matrix products, arithmetic and copies ran while one was open for 15% -> 27% of each run, Pallas kernels for 0% -> 0%
where the time goes in v1:
time: 190 us
  waiting for transfers between devices  106 us (56%)
  matrix products  34.3 us (18%)
  other arithmetic  19.4 us (10%)
  between operations  14.1 us (7%)
  local copies, waits for them, and re-layouts  9.77 us (5%)
  starting transfers between devices  3.58 us (2%)
  loops' own time  3.07 us (2%)
    all_gather x1, waiting for transfers between devices, per_device(): lax.all_gather(key_rows, 'sp', axis=0, tiled=True)  35 us
    all_gather x1, waiting for transfers between devices, per_device(): lax.all_gather(values, 'sp', axis=0, tiled=True)  28.9 us
    all_gather x1, waiting for transfers between devices, per_device(): lax.all_gather(tokens, 'tp', axis=1, tiled=True)  26.6 us
    dot_general x4, matrix products, block_scores(): jnp.einsum('qhcd,khcd->hcqk', queries, key_block, preferred_element_type=...  17.6 us
    all_gather x1, waiting for transfers between devices, per_device(): lax.all_gather(attn_out, 'tp', axis=1, tiled=True)  13.4 us
    dot_general x6, matrix products, add_products(): jnp.dot(scaled, weight, preferred_element_type=jnp.float32)  10.6 us
    reduce_sum x2, other arithmetic, stats_step(): jnp.sum(exponent, axis=-1)  8.38 us
  transfers between devices with their start and end apart: 6, of which 5 were waited for; matrix products, arithmetic and copies ran while one was open for 27% of the time, Pallas kernels for 0%

profile of v1, /device:TPU:0, one launch (start us, length us, event | category | flops | bytes accessed | tf_op | source)
XLA Modules:
  0.0 190.0 jit_solution(15616992371786437364)
XLA Ops:
  7.2 0.0 copy-start
  7.2 0.0 copy-start.13
  7.2 0.0 all-gather.7.cloned.1.call-start
  7.2 0.7 all-gather.7.cloned.1.call-update
  7.9 0.0 all-gather.11.cloned.1.call-start
  8.0 0.3 multiply_cosine_fusion
  8.3 26.6 %all-gather.7.cloned.1.call-done = bf16[512,2048]{1,0:T(8,128)(2,1)} async-done(((bf16[512,512]{1,0:T(8,128)(2,1)}), bf16[512,2048]{1,0:T(8,128)(2,1)}) %all-gather.7.cloned.1.call-update) | async-done | bytes 2097168 | tf_op jit(solution)/shard_map/all_gather | solution.py:90
  34.9 2.2 %fusion.32 = f32[512]{0:T(512)S(1)} fusion(bf16[512,2048]{1,0:T(8,128)(2,1)} %all-gather.7.cloned.1.call-done), kind=kLoop, calls=%fused_computation.40 | loop fusion | flops 3145216 | bytes 2099200 | tf_op jit(solution)/shard_map/reduce_sum | solution.py:43
  37.1 2.6 %convolution_multiply_fusion.4 = f32[512,256]{0,1:T(8,128)S(1)} fusion(bf16[2048,256]{1,0:T(8,128)(2,1)} %param.20, bf16[512,2048]{1,0:T(8,128)(2,1)} %all-gather.7.cloned.1.call-done, f32[2048]{0:T(1024)} %param.18, f32[512]{0:T(512)S(1)} %add_rsqrt_fusion.1), kind=kOutput, calls=%fused_computation.49 | convolution fusion | flops 540147712 | bytes 3680256 | tf_op jit(solution)/shard_map/dot_general | solution.py:41
  39.8 0.8 convolution_multiply_fusion.3
  40.6 0.2 subtract_convert_fusion
  40.8 0.7 pad_maximum_fusion.1
  41.5 0.0 all-gather.11.cloned.1.call-update
  41.5 0.0 copy-start.14
  41.5 0.0 all-gather.9.cloned.1.call-start
  41.6 2.7 %fusion.35 = bf16[512,256]{0,1:T(8,128)(2,1)} fusion(bf16[2048,256]{1,0:T(8,128)(2,1)} %param.21, bf16[512,2048]{1,0:T(8,128)(2,1)S(1)} %copy-done.1, f32[2048]{0:T(1024)S(1)} %copy-done.13, f32[512]{0:T(512)S(1)} %add_rsqrt_fusion.1), kind=kOutput, calls=%fused_computation.51 | convolution fusion | flops 540278784 | bytes 3418112 | tf_op jit(solution)/shard_map/dot_general | solution.py:41
  44.3 1.8 copy.22
  46.1 0.0 all-gather.9.cloned.1.call-update
  46.1 0.0 all-gather.15.cloned.1.call-start
  46.2 0.8 fusion.53
  47.0 2.1 %fusion.42 = f32[512,256]{0,1:T(8,128)S(1)} fusion(bf16[2048,256]{1,0:T(8,128)(2,1)} %param.23, bf16[512,2048]{1,0:T(8,128)(2,1)S(1)} %copy-done.1, f32[2048]{0:T(1024)} %param.18, f32[512]{0:T(512)} %copy-done.5), kind=kOutput, calls=%fused_computation.58 | convolution fusion | flops 540409856 | bytes 3680256 | tf_op jit(solution)/shard_map/dot_general | solution.py:41
  49.1 0.8 fusion.41
  49.9 0.1 slice.54
  50.0 3.4 %collective-permute-start = (bf16[2,256]{0,1:T(8,128)(2,1)S(1)}, bf16[2,256]{0,1:T(8,128)(2,1)S(1)}, u32[]{:S(2)}, u32[]{:S(2)}) collective-permute-start(bf16[2,256]{0,1:T(8,128)(2,1)S(1)} %slice.54), channel_id=1, source_target_pairs={{0,4},{4,8},{8,12},{12,16},{16,20},{20,24},{24,28},{1,5},{5,9},{9,... | collective-permute-start | bytes 3080 | tf_op jit(solution)/shard_map/ppermute | solution.py:17
  53.4 0.7 pad_maximum_fusion.2
  54.1 1.2 collective-permute-done
  55.3 1.6 fusion.45
  56.9 0.0 all-gather.15.cloned.1.call-update
  56.9 0.0 all-gather.13.cloned.1.call-start
  57.0 35.0 %all-gather.11.cloned.1.call-done = bf16[4096,2,2,64]{0,3,2,1:T(8,128)(2,1)} async-done(((bf16[512,2,2,64]{0,3,2,1:T(8,128)(2,1)}), bf16[4096,2,2,64]{0,3,2,1:T(8,128)(2,1)}) %all-gather.11.cloned.1.call-update) | async-done | bytes 2097168 | tf_op jit(solution)/shard_map/all_gather | solution.py:162
  92.0 1.7 copy.40
  93.7 0.0 copy-start.15
  93.7 18.8 %while.24 = (s32[]{:T(128)}, f32[2,2,512]{2,1,0:T(2,128)S(1)}, f32[2,2,512]{2,1,0:T(2,128)S(1)}, s32[2]{0:T(128)S(1)}, bf16[2,2048,2,2,64]{1,4,3,2,0:T(8,128)(2,...) while((s32[]{:T(128)}, f32[2,2,512]{2,1,0:T(2,128)S(1)}, ...), condition=%wide.region_4.5_spmd.clone, body=%wide.region_1.4_spmd.clone.sunk | while | flops 571486720 | bytes 38138008 | solution.py:59
  93.9 0.6 dynamic_slice.43
  95.2 0.8 broadcast_compare_fusion.4
  96.0 3.0 %fusion.78 = (f32[2,2,512]{2,1,0:T(2,128)S(1)}, f32[2,2,2048,512]{3,2,1,0:T(8,128)S(1)}) fusion(pred[512,2048]{0,1:T(8,128)(4,1)S(1)} %broadcast_compare_fusion.4, bf16[512,2,2,64]{0,3,2,1:T(8,128)(2,1)S(1)} %get-tuple-element.355, bf16[2,2048,2,2,64]{1,4,3,2,0:T(8,128)(2,1)S(1)} %get-tuple-element.354, s32[]{:T(128)S(6)} %copy.45), kind=kOutput, calls=%fused_computation.4.clone.1 | convolution fusion | flops 549451776 | bytes 19144708 | tf_op jit(solution)/shard_map/while/body/eval_jaxpr/qhcd,khcd->hcqk/dot_general | solution.py:120
  99.0 4.2 %select_reduce_fusion.2 = f32[2,2,512]{2,1,0:T(2,128)S(1)} fusion(f32[2,2,2048,512]{3,2,1,0:T(8,128)S(1)} %get-tuple-element.319, f32[2,2,512]{2,1,0:T(2,128)S(1)} %fusion.79, pred[512,2048]{0,1:T(8,128)(4,1)S(1)} %broadcast_compare_fusion.4), kind=kLoop, calls=%fused_computation.3.clone.1 | loop fusion | flops 20969472 | bytes 17842176 | tf_op jit(solution)/shard_map/while/body/eval_jaxpr/reduce_sum | solution.py:136
  103.2 0.6 dynamic_slice.43
  104.5 0.8 broadcast_compare_fusion.4
  105.3 3.0 %fusion.78 = (f32[2,2,512]{2,1,0:T(2,128)S(1)}, f32[2,2,2048,512]{3,2,1,0:T(8,128)S(1)}) fusion(pred[512,2048]{0,1:T(8,128)(4,1)S(1)} %broadcast_compare_fusion.4, bf16[512,2,2,64]{0,3,2,1:T(8,128)(2,1)S(1)} %get-tuple-element.355, bf16[2,2048,2,2,64]{1,4,3,2,0:T(8,128)(2,1)S(1)} %get-tuple-element.354, s32[]{:T(128)S(6)} %copy.45), kind=kOutput, calls=%fused_computation.4.clone.1 | convolution fusion | flops 549451776 | bytes 19144708 | tf_op jit(solution)/shard_map/while/body/eval_jaxpr/qhcd,khcd->hcqk/dot_general | solution.py:120
  108.3 4.2 %select_reduce_fusion.2 = f32[2,2,512]{2,1,0:T(2,128)S(1)} fusion(f32[2,2,2048,512]{3,2,1,0:T(8,128)S(1)} %get-tuple-element.319, f32[2,2,512]{2,1,0:T(2,128)S(1)} %fusion.79, pred[512,2048]{0,1:T(8,128)(4,1)S(1)} %broadcast_compare_fusion.4), kind=kLoop, calls=%fused_computation.3.clone.1 | loop fusion | flops 20969472 | bytes 17842176 | tf_op jit(solution)/shard_map/while/body/eval_jaxpr/reduce_sum | solution.py:136
  112.5 28.9 %all-gather.9.cloned.1.call-done = bf16[4096,2,128]{2,0,1:T(8,128)(2,1)} async-done(((bf16[512,2,128]{2,0,1:T(8,128)(2,1)}), bf16[4096,2,128]{2,0,1:T(8,128)(2,1)}) %all-gather.9.cloned.1.call-update) | async-done | bytes 2097168 | tf_op jit(solution)/shard_map/all_gather | solution.py:163
  141.5 20.0 %while.25 = (s32[]{:T(128)}, f32[512,2,128]{0,2,1:T(8,128)}, bf16[2,2048,2,128]{3,1,0,2:T(8,128)(2,1)}, s32[2]{0:T(128)S(1)}, bf16[2,2048,2,2,64]{1,4,3,2,0:T(8,...) while((s32[]{:T(128)}, f32[512,2,128]{0,2,1:T(8,128)}, ...), condition=%wide.region_6.7_spmd.clone, body=%wide.region_5.6_spmd.clone.sunk | while | flops 1102318080 | bytes 51680008 | solution.py:59
  141.5 0.6 dynamic_slice.46
  142.7 0.8 broadcast_compare_fusion.5
  143.5 0.0 copy-start.2
  143.5 5.8 %fusion.85 = f32[2,2,512,2048]{2,3,1,0:T(8,128)S(1)} fusion(f32[2,2,512]{2,1,0:T(2,128)S(1)} %get-tuple-element.393, f32[2,2,512]{2,1,0:T(2,128)S(1)} %get-tuple-element.392, pred[512,2048]{0,1:T(8,128)(4,1)S(1)} %broadcast_compare_fusion.5, bf16[512,2,2,64]{0,3,2,1:T(8,128)(2,1)S(1)} %get-tuple-element.391, ...), kind=kOutput, calls=%fused_computation.20.clone.1 | convolution fusion | flops 557842432 | bytes 19152900 | tf_op jit(solution)/shard_map/while/body/eval_jaxpr/qhcd,khcd->hcqk/dot_general | solution.py:120
  149.4 1.3 fusion.86
  150.7 0.0 copy-start.3
  150.7 0.8 copy-done.3
  151.5 0.6 dynamic_slice.46
  152.7 0.8 broadcast_compare_fusion.5
  153.5 5.8 %fusion.85 = f32[2,2,512,2048]{2,3,1,0:T(8,128)S(1)} fusion(f32[2,2,512]{2,1,0:T(2,128)S(1)} %get-tuple-element.393, f32[2,2,512]{2,1,0:T(2,128)S(1)} %get-tuple-element.392, pred[512,2048]{0,1:T(8,128)(4,1)S(1)} %broadcast_compare_fusion.5, bf16[512,2,2,64]{0,3,2,1:T(8,128)(2,1)S(1)} %get-tuple-element.391, ...), kind=kOutput, calls=%fused_computation.20.clone.1 | convolution fusion | flops 557842432 | bytes 19152900 | tf_op jit(solution)/shard_map/while/body/eval_jaxpr/qhcd,khcd->hcqk/dot_general | solution.py:120
  159.4 1.3 fusion.86
  160.7 0.8 copy-done.3
  161.5 1.1 multiply_reduce_fusion
  162.6 2.0 %multiply_convert_fusion = bf16[512,2,128]{0,2,1:T(8,128)(2,1)} fusion(f32[512,2,128]{0,2,1:T(8,128)} %get-tuple-element.94, f32[128]{0:T(128)S(1)} %copy-done.7, f32[512,2]{0,1:T(2,128)S(1)} %add_rsqrt_fusion), kind=kLoop, calls=%fused_computation.63 | loop fusion | flops 524288 | bytes 791040 | tf_op jit(solution)/shard_map/convert_element_type | solution.py:176
  164.6 0.0 all-gather.13.cloned.1.call-update
  164.6 0.0 all-gather.15.cloned.1.call-done
  164.6 1.3 copy.41
  165.9 0.6 log_add_fusion
  166.6 13.4 %all-gather.13.cloned.1.call-done = bf16[512,1024]{0,1:T(8,128)(2,1)} async-done(((bf16[512,256]{0,1:T(8,128)(2,1)}), bf16[512,1024]{0,1:T(8,128)(2,1)}) %all-gather.13.cloned.1.call-update) | async-done | bytes 1048592 | tf_op jit(solution)/shard_map/all_gather | solution.py:179
  180.0 2.0 %fusion.54 = f32[512,512]{1,0:T(8,128)S(1)} fusion(bf16[512,1024]{0,1:T(8,128)(2,1)} %all-gather.13.cloned.1.call-done, bf16[1024,512]{1,0:T(8,128)(2,1)S(1)} %copy-done), kind=kOutput, calls=%fused_computation.83 | convolution fusion | flops 536870912 | bytes 3145728 | tf_op jit(solution)/shard_map/dot_general | solution.py:178
  181.9 1.5 fusion.34
  (53 shorter events, 0.2 us)
Async XLA Ops:
  7.2 172.8 %copy-start = (bf16[1024,512]{1,0:T(8,128)(2,1)S(1)}, bf16[1024,512]{1,0:T(8,128)(2,1)}, u32[]{:S(2)}) copy-start(bf16[1024,512]{1,0:T(8,128)(2,1)} %param.28) | copy-start | bytes 3145732
  7.2 32.6 %copy-start.13 = (f32[2048]{0:T(1024)S(1)}, f32[2048]{0:T(1024)}, u32[]{:S(2)}) copy-start(f32[2048]{0:T(1024)} %param.18) | copy-start | bytes 24580
  7.2 27.7 %all-gather.7.cloned.1.call-start = ((), (), s32[]{:S(2)}) async-start(), calls=%async_computation | async-start | bytes 2621440 | tf_op jit(solution)/shard_map/all_gather | solution.py:90
  7.9 84.0 %all-gather.11.cloned.1.call-start = ((), (), s32[]{:S(2)}) async-start(), calls=%async_computation.2 | async-start | bytes 2359296 | tf_op jit(solution)/shard_map/all_gather | solution.py:162
  34.9 4.9 %copy-start.1 = (bf16[512,2048]{1,0:T(8,128)(2,1)S(1)}, bf16[512,2048]{1,0:T(8,128)(2,1)}, u32[]{:S(2)}) copy-start(bf16[512,2048]{1,0:T(8,128)(2,1)} %all-gather.7.cloned.1.call-done) | copy-start | bytes 6291460
  34.9 4.9 %copy-start.9 = (bf16[2048,256]{1,0:T(8,128)(2,1)S(1)}, bf16[2048,256]{1,0:T(8,128)(2,1)}, u32[]{:S(2)}) copy-start(bf16[2048,256]{1,0:T(8,128)(2,1)} %param.19) | copy-start | bytes 3145732
  37.1 4.5 %copy-start.5 = (f32[512]{0:T(512)}, f32[512]{0:T(512)S(1)}, u32[]{:S(2)}) copy-start(f32[512]{0:T(512)S(1)} %add_rsqrt_fusion.1) | copy-start | bytes 6148
  41.5 7.6 %copy-start.14 = (f32[2048]{0:T(1024)S(1)}, f32[2048]{0:T(1024)}, u32[]{:S(2)}) copy-start(f32[2048]{0:T(1024)} %param.18) | copy-start | bytes 24580
  41.5 99.9 %all-gather.9.cloned.1.call-start = ((), (), s32[]{:S(2)}) async-start(), calls=%async_computation.1 | async-start | bytes 2359296 | tf_op jit(solution)/shard_map/all_gather | solution.py:163
  44.3 4.8 %copy-start.6 = (f32[512]{0:T(512)S(1)}, f32[512]{0:T(512)}, u32[]{:S(2)}) copy-start(f32[512]{0:T(512)} %copy-done.5) | copy-start | bytes 6148
  46.1 118.5 %all-gather.15.cloned.1.call-start = ((), (), s32[]{:S(2)}) async-start(), calls=%async_computation.4 | async-start | bytes 1310720 | tf_op jit(solution)/shard_map/all_gather | solution.py:184
  46.2 2.9 %copy-start.10 = (bf16[2048,256]{1,0:T(8,128)(2,1)S(1)}, bf16[2048,256]{1,0:T(8,128)(2,1)}, u32[]{:S(2)}) copy-start(bf16[2048,256]{1,0:T(8,128)(2,1)} %param.24) | copy-start | bytes 3145732
  47.0 8.3 %copy-start.11 = (bf16[2048,256]{1,0:T(8,128)(2,1)S(1)}, bf16[2048,256]{1,0:T(8,128)(2,1)}, u32[]{:S(2)}) copy-start(bf16[2048,256]{1,0:T(8,128)(2,1)} %param.22) | copy-start | bytes 3145732
  50.0 5.3 %collective-permute-start = (bf16[2,256]{0,1:T(8,128)(2,1)S(1)}, bf16[2,256]{0,1:T(8,128)(2,1)S(1)}, u32[]{:S(2)}, u32[]{:S(2)}) collective-permute-start(bf16[2,256]{0,1:T(8,128)(2,1)S(1)} %slice.54), channel_id=1, source_target_pairs={{0,4},{4,8},{8,12},{12,16},{16,20},{20,24},{24,28},{1,5},{5,9},{9,... | collective-permute-start | bytes 3080 | tf_op jit(solution)/shard_map/ppermute | solution.py:17
  55.3 38.4 %copy-start.4 = (bf16[512,2,2,64]{0,3,2,1:T(8,128)(2,1)S(1)}, bf16[512,2,2,64]{0,3,2,1:T(8,128)(2,1)}, u32[]{:S(2)}) copy-start(bf16[512,2,2,64]{0,3,2,1:T(8,128)(2,1)} %pad_maximum_fusion.2) | copy-start | bytes 786436
  56.9 123.0 %all-gather.13.cloned.1.call-start = ((), (), s32[]{:S(2)}) async-start(), calls=%async_computation.3 | async-start | bytes 1310720 | tf_op jit(solution)/shard_map/all_gather | solution.py:179
  93.7 47.7 %copy-start.15 = (f32[2]{0:T(128)S(1)}, f32[2]{0:T(128)}, u32[]{:S(2)}) copy-start(f32[2]{0:T(128)} %param.26) | copy-start | bytes 28
  141.4 21.1 %copy-start.7 = (f32[128]{0:T(128)S(1)}, f32[128]{0:T(128)}, u32[]{:S(2)}) copy-start(f32[128]{0:T(128)} %param.27) | copy-start | bytes 1540
  143.5 5.9 %copy-start.2 = (f32[512,2,128]{0,2,1:T(8,128)S(1)}, f32[512,2,128]{0,2,1:T(8,128)}, u32[]{:S(2)}) copy-start(f32[512,2,128]{0,2,1:T(8,128)} %get-tuple-element.374) | copy-start | bytes 1572868 | tf_op jit(solution)/shard_map/while
  143.5 5.9 %copy-start.8 = (bf16[2,2048,2,128]{3,1,0,2:T(8,128)(2,1)S(1)}, bf16[2,2048,2,128]{3,1,0,2:T(8,128)(2,1)}, u32[]{:S(2)}) copy-start(bf16[2,2048,2,128]{3,1,0,2:T(8,128)(2,1)} %get-tuple-element.388) | copy-start | bytes 6291460 | tf_op jit(solution)/shard_map/while
  150.7 0.8 copy-start.3
  153.5 5.9 %copy-start.2 = (f32[512,2,128]{0,2,1:T(8,128)S(1)}, f32[512,2,128]{0,2,1:T(8,128)}, u32[]{:S(2)}) copy-start(f32[512,2,128]{0,2,1:T(8,128)} %get-tuple-element.374) | copy-start | bytes 1572868 | tf_op jit(solution)/shard_map/while
  153.5 5.9 %copy-start.8 = (bf16[2,2048,2,128]{3,1,0,2:T(8,128)(2,1)S(1)}, bf16[2,2048,2,128]{3,1,0,2:T(8,128)(2,1)}, u32[]{:S(2)}) copy-start(bf16[2,2048,2,128]{3,1,0,2:T(8,128)(2,1)} %get-tuple-element.388) | copy-start | bytes 6291460 | tf_op jit(solution)/shard_map/while
  160.7 0.8 copy-start.3
  162.6 19.3 %copy-start.12 = (bf16[1024,512]{1,0:T(8,128)(2,1)S(1)}, bf16[1024,512]{1,0:T(8,128)(2,1)}, u32[]{:S(2)}) copy-start(bf16[1024,512]{1,0:T(8,128)(2,1)} %param.29) | copy-start | bytes 3145732
Sparse Core Ops, SparseCore 0:
  9.6 25.2 all-gather.6
  41.6 50.2 all-gather.10
  94.2 47.2 all-gather.8
  142.9 15.2 all-gather.14
  164.7 15.2 all-gather.12
